TPU v7x, 32 devices: a whole 2x2x4 slice. The times are simulated.
32 devices in a mesh: ep: 8 (over z, core), tp: 4 (over y, x).
Axes of the slice: x: 2, y: 2, z: 4, core: 2. Of those that a mesh axis runs over, the one named last changes fastest.
Arguments:
- mix_input: bfloat16 [1024, 2048], P('ep'), may hold values from -8 to 8
- expert_input: bfloat16 [1024, 2048], P('ep'), may hold values from -8 to 8
- mix_gain: float32 [2048], replicated, may hold values from 0.1 to 1.9
- moe_gain: float32 [2048], replicated, may hold values from 0.1 to 1.9
- pool_in: bfloat16 [2048, 1024], P(None, 'tp'), may hold values from -0.125 to 0.125
- pool_scale: float32 [1024], P('tp'), may hold values from 0.25 to 10
- pool_gain: float32 [1024], P('tp'), may hold values from 0.1 to 1.9
- pool_out: bfloat16 [1024, 2048], P(None, 'tp'), may hold values from -0.1875 to 0.1875
- route: int32 [1024, 4], P('ep'), may hold values from 0 to 7, all different within a row; in each aligned block of 128 rows (0 to 127, 128 to 255, ...) at most 128 rows name the same one
- route_score: float32 [1024, 4], P('ep'), may hold values from 0.05 to 1
- expert_gate: bfloat16 [8, 2048, 2048], P('ep', None, 'tp'), may hold values from -0.125 to 0.125
- expert_up: bfloat16 [8, 2048, 2048], P('ep', None, 'tp'), may hold values from -0.125 to 0.125
- expert_down: bfloat16 [8, 2048, 2048], P('ep', 'tp'), may hold values from -0.1875 to 0.1875
- shared_gate: bfloat16 [2048, 2048], P(None, 'tp'), may hold values from -0.125 to 0.125
- shared_up: bfloat16 [2048, 2048], P(None, 'tp'), may hold values from -0.125 to 0.125
- shared_down: bfloat16 [2048, 2048], P(None, 'tp'), may hold values from -0.125 to 0.125
Outputs:
- mix_out: bfloat16 [1024, 2048], P('ep', 'tp')
- moe_out: bfloat16 [1024, 2048], P('ep', 'tp')
Inputs may be any that keep to these rules, and one draw needn't show every extreme that they name: `route`: each row names 4 different experts. In the rows of one index of ep (aligned blocks of 128 rows) no expert is named more than 128 times, a bound that some block reaches.
All inputs are finite; a program needn't handle non-finite values.
Results may differ from a plain program's by a relative error of at most 0.014.
Values may be sent and summed in bfloat16 or wider, within the bound.
No kernel may reach another device: no remote copies, remote signals or barrier semaphores. Data moves between devices by JAX's collectives and lax.ppermute only.
A program may use at most 64 MiB of HBM per device.

v0:
```python
import jax
import jax.numpy as jnp
from jax import lax
from jax.sharding import PartitionSpec as P

epsilon = 1e-06
reach_rows = 15
window_widths = (2, 4, 8, 16)


def shifted(block, axis, distance):
    devices = range(lax.axis_size(axis))
    route = [(i - distance, i) for i in devices if i - distance in devices]
    return lax.ppermute(block, axis, route)


def row_norm(rows, gain):
    values = rows.astype(jnp.float32)
    scale = lax.rsqrt(jnp.mean(values * values, axis=-1, keepdims=True) + epsilon)
    return (values * scale * gain).astype(jnp.bfloat16)


def window_means(extended, position, group, n_rows):
    total = jnp.zeros((n_rows, extended.shape[1]), jnp.float32)
    result = jnp.zeros((n_rows, extended.shape[1]), jnp.float32)
    for lag in range(16):
        total = total + extended[reach_rows - lag : reach_rows - lag + n_rows]
        for index, width in enumerate(window_widths):
            if lag + 1 == width:
                count = jnp.minimum(position, float(width))[:, None]
                result = jnp.where(group[None, :] == index, total / count, result)
    return result - extended[reach_rows:]


def serve(sending, expert_gate, expert_up, expert_down):
    arrived = lax.all_to_all(sending, "ep", split_axis=0, concat_axis=0, tiled=True)
    gate = jnp.einsum("send,edf->senf", arrived, expert_gate, preferred_element_type=jnp.float32)
    upper = jnp.einsum("send,edf->senf", arrived, expert_up, preferred_element_type=jnp.float32)
    hidden = (jax.nn.silu(gate) * upper).astype(jnp.bfloat16)
    term = jnp.einsum("senf,efd->send", hidden, expert_down, preferred_element_type=jnp.float32)
    summed = lax.psum_scatter(term.astype(jnp.bfloat16), "tp", scatter_dimension=3, tiled=True)
    return lax.all_to_all(summed, "ep", split_axis=0, concat_axis=0, tiled=True)


def on_device(
    mix_input,
    expert_input,
    mix_gain,
    moe_gain,
    pool_in,
    pool_scale,
    pool_gain,
    pool_out,
    route,
    route_score,
    expert_gate,
    expert_up,
    expert_down,
    shared_gate,
    shared_up,
    shared_down,
):
    tok_rows = mix_input.shape[0]
    channels = pool_in.shape[1]
    pool_width = channels * lax.axis_size("tp")
    mix_norm = row_norm(mix_input, mix_gain)
    pool_input = jnp.dot(mix_norm, pool_in, preferred_element_type=jnp.float32).astype(jnp.bfloat16)
    before = shifted(pool_input[tok_rows - reach_rows :], "ep", 1)
    extended = jnp.concatenate([before, pool_input], axis=0).astype(jnp.float32)
    position = (lax.axis_index("ep") * tok_rows + jnp.arange(tok_rows, dtype=jnp.int32) + 1).astype(
        jnp.float32
    )
    channel_ids = lax.axis_index("tp") * channels + jnp.arange(channels, dtype=jnp.int32)
    group = channel_ids // (pool_width // 4)
    scaled = window_means(extended, position, group, tok_rows) * pool_scale
    squares = lax.psum(jnp.sum(scaled * scaled, axis=1), "tp")
    pooled_norm = (scaled * lax.rsqrt(squares / pool_width + epsilon)[:, None] * pool_gain).astype(
        jnp.bfloat16
    )
    moe_norm = row_norm(expert_input, moe_gain)
    shared_hidden = (
        jax.nn.silu(jnp.dot(moe_norm, shared_gate, preferred_element_type=jnp.float32))
        * jnp.dot(moe_norm, shared_up, preferred_element_type=jnp.float32)
    ).astype(jnp.bfloat16)
    pooled_all, shared_all = (
        lax.all_gather(pooled_norm, "tp", axis=1, tiled=True),
        lax.all_gather(shared_hidden, "tp", axis=1, tiled=True),
    )
    mix_out = jnp.dot(pooled_all, pool_out, preferred_element_type=jnp.float32).astype(jnp.bfloat16)
    shared_part = jnp.dot(shared_all, shared_down, preferred_element_type=jnp.float32)
    n_tok, top = route.shape
    local_experts = expert_gate.shape[0]
    experts = local_experts * lax.axis_size("ep")
    capacity = 2 * n_tok * top // experts
    flat_route = route.reshape(-1)
    table = (flat_route[:, None] == jnp.arange(experts, dtype=jnp.int32)[None, :]).astype(jnp.int32)
    ranks = jnp.sum((jnp.cumsum(table, axis=0) - table) * table, axis=1)
    slot = flat_route * capacity + ranks
    owner = (
        jnp.full((experts * capacity,), n_tok, jnp.int32)
        .at[slot]
        .set(jnp.arange(n_tok * top, dtype=jnp.int32) // top)
    )
    padded_rows = jnp.concatenate(
        [moe_norm, jnp.zeros((1, moe_norm.shape[1]), jnp.bfloat16)], axis=0
    )
    outgoing = padded_rows[owner].reshape(
        lax.axis_size("ep"), local_experts, capacity, moe_norm.shape[1]
    )
    middle = capacity // 2
    first = serve(outgoing[:, :, :middle], expert_gate, expert_up, expert_down)
    second = serve(outgoing[:, :, middle:], expert_gate, expert_up, expert_down)
    returned = jnp.concatenate([first, second], axis=2)
    back_rows = returned.reshape(experts * capacity, returned.shape[3])
    picked = back_rows[slot].reshape(n_tok, top, returned.shape[3]).astype(jnp.float32)
    weights = 2.5 * route_score / jnp.sum(route_score, axis=1, keepdims=True)
    routed = jnp.sum(picked * weights[:, :, None], axis=1)
    moe_out = (routed + shared_part).astype(jnp.bfloat16)
    return (mix_out, moe_out)


def solution(mesh):
    return jax.shard_map(
        on_device,
        mesh=mesh,
        in_specs=(
            P("ep", None),
            P("ep", None),
            P(),
            P(),
            P(None, "tp"),
            P("tp"),
            P("tp"),
            P(None, "tp"),
            P("ep", None),
            P("ep", None),
            P("ep", None, "tp"),
            P("ep", None, "tp"),
            P("ep", "tp", None),
            P(None, "tp"),
            P(None, "tp"),
            P(None, "tp"),
        ),
        out_specs=(P("ep", "tp"), P("ep", "tp")),
        check_vma=False,
    )
```

profile of v0, /device:TPU:0, one launch (start us, length us, event | category | flops | bytes accessed | tf_op | source)
XLA Modules:
  0.0 223.1 jit_solution(1596162430017472814)
XLA Ops:
  7.2 0.9 copy.24
  8.3 0.7 broadcast_multiply_fusion
  9.0 1.1 reduce-window.6
  10.8 2.4 %scatter_custom_fusion = s32[1024]{0:T(1024)S(1)} fusion(s32[512]{0:T(512)S(1)} %bitcast.166, s32[512]{0:T(512)S(1)} %add_select_fusion, s32[]{:T(128)} %constant.80.clone.1), kind=kCustom, calls=%fused_computation.93 | custom fusion | bytes 4100 | tf_op jit(solution)/shard_map/scatter | solution.py:102
  13.2 1.2 fusion.71
  14.5 1.2 fusion.73
  15.8 6.0 %gather_fusion = bf16[1024,2048]{1,0:T(8,128)(2,1)} fusion(bf16[129,2048]{1,0:T(8,128)(2,1)S(1)} %concatenate.10, s32[1024]{0:T(1024)S(1)} %fusion.94), kind=kCustom, calls=%fused_computation | custom fusion | bytes 8392704 | tf_op jit(solution)/shard_map/gather | solution.py:107
  21.8 4.1 %fusion.103 = (bf16[8,1,64,2048]{3,2,1,0:T(8,128)(2,1)S(1)}, bf16[8,1,64,2048]{3,2,1,0:T(8,128)(2,1)}) fusion(bf16[8,1,128,2048]{3,2,1,0:T(8,128)(2,1)} %bitcast.163), kind=kLoop, calls=%fused_computation.115 | loop fusion | bytes 8388608 | tf_op jit(solution)/shard_map/slice | solution.py:111
  25.9 55.3 %all_to_all.20 = bf16[8,1,64,2048]{3,2,1,0:T(8,128)(2,1)} all-to-all(bf16[8,1,64,2048]{3,2,1,0:T(8,128)(2,1)S(1)} %get-tuple-element.4), channel_id=1, replica_groups=mesh['ep'=8,'tp'=4] {'ep'}, dimensions={0} | all-to-all | bytes 4194304 | tf_op jit(solution)/shard_map/all_to_all | solution.py:36
  81.2 4.4 %all-to-all-start.2 = ((bf16[8,1,64,2048]{3,2,1,0:T(8,128)(2,1)}), bf16[8,1,64,2048]{3,2,1,0:T(8,128)(2,1)}, u32[]{:S(2)}, u32[]{:S(2)}) async-start(bf16[8,1,64,2048]{3,2,1,0:T(8,128)(2,1)} %get-tuple-element.5), calls=%async_computation.3 | async-start | bytes 4194304 | tf_op jit(solution)/shard_map/all_to_all | solution.py:36
  85.6 4.5 %fusion.16 = f32[8,1,64,512]{3,2,0,1:T(8,128)} fusion(bf16[1,2048,512]{2,1,0:T(8,128)(2,1)} %param.26, bf16[8,1,64,2048]{3,2,1,0:T(8,128)(2,1)} %all_to_all.20), kind=kOutput, calls=%fused_computation.21 | convolution fusion | flops 1073741824 | bytes 5242880 | tf_op jit(solution)/shard_map/send,edf->senf/dot_general | solution.py:37
  90.1 6.3 %fusion = bf16[8,1,64,2048]{3,2,0,1:T(8,128)(2,1)} fusion(bf16[1,512,2048]{2,1,0:T(8,128)(2,1)S(1)} %copy-done, bf16[1,2048,512]{2,1,0:T(8,128)(2,1)} %param.27, bf16[8,1,64,2048]{3,2,1,0:T(8,128)(2,1)} %all_to_all.20, f32[8,1,64,512]{3,2,0,1:T(8,128)} %fusion.16), kind=kOutput, calls=%fused_computation.5 | convolution fusion | flops 2150105088 | bytes 9437184 | tf_op jit(solution)/shard_map/senf,efd->send/dot_general | solution.py:40
  96.5 38.1 %all-to-all-done.2 = bf16[8,1,64,2048]{3,2,1,0:T(8,128)(2,1)} async-done(((bf16[8,1,64,2048]{3,2,1,0:T(8,128)(2,1)}), bf16[8,1,64,2048]{3,2,1,0:T(8,128)(2,1)}, u32[]{:S(2)}, u32[]{:S(2)}) %all-to-all-start.2) | async-done | bytes 2097184 | tf_op jit(solution)/shard_map/all_to_all | solution.py:36
  134.6 4.5 %fusion.31 = f32[8,1,64,512]{3,2,0,1:T(8,128)} fusion(bf16[1,2048,512]{2,1,0:T(8,128)(2,1)} %param.26, bf16[8,1,64,2048]{3,2,1,0:T(8,128)(2,1)} %all-to-all-done.2), kind=kOutput, calls=%fused_computation.24 | convolution fusion | flops 1073741824 | bytes 5242880 | tf_op jit(solution)/shard_map/send,edf->senf/dot_general | solution.py:37
  139.1 6.2 %fusion.1 = bf16[8,1,64,2048]{3,2,0,1:T(8,128)(2,1)} fusion(bf16[1,512,2048]{2,1,0:T(8,128)(2,1)S(1)} %copy-done, bf16[1,2048,512]{2,1,0:T(8,128)(2,1)} %param.27, bf16[8,1,64,2048]{3,2,1,0:T(8,128)(2,1)} %all-to-all-done.2, f32[8,1,64,512]{3,2,0,1:T(8,128)} %fusion.31), kind=kOutput, calls=%fused_computation.6 | convolution fusion | flops 2150105088 | bytes 9437184 | tf_op jit(solution)/shard_map/senf,efd->send/dot_general | solution.py:40
  145.3 1.0 copy-done.2
  146.5 1.6 convolution_convert_fusion.3
  148.1 1.4 collective-permute-start
  149.7 3.5 %all-to-all-start.1 = ((bf16[8,1,64,512]{3,2,1,0:T(8,128)(2,1)}), bf16[8,1,64,512]{3,2,1,0:T(8,128)(2,1)S(1)}, u32[]{:S(2)}, u32[]{:S(2)}) async-start(bf16[8,1,64,512]{3,2,1,0:T(8,128)(2,1)} %bitcast.165), calls=%async_computation.2 | async-start | bytes 1048576 | tf_op jit(solution)/shard_map/all_to_all | solution.py:42
  153.3 2.2 fusion.104
  155.5 0.5 fusion.66
  156.0 13.6 %all_gather.7 = bf16[128,2048]{1,0:T(8,128)(2,1)} all-gather(bf16[128,512]{1,0:T(8,128)(2,1)S(1)} %fusion.66), channel_id=1, replica_groups=mesh['ep'=8,'tp'=4] {'tp'}, dimensions={1}, use_global_device_ids=true | all-gather | bytes 655360 | tf_op jit(solution)/shard_map/all_gather | solution.py:87
  169.7 11.3 %reduce-scatter.5.cloned.1.call-done = bf16[8,1,64,512]{3,2,0,1:T(8,128)(2,1)} async-done(((bf16[8,1,64,2048]{3,2,0,1:T(8,128)(2,1)}), bf16[8,1,64,512]{3,2,0,1:T(8,128)(2,1)}) %reduce-scatter.5.cloned.1.call-update) | async-done | bytes 524304 | tf_op jit(solution)/shard_map/reduce_scatter | solution.py:41
  181.0 4.6 %all-to-all-start.3 = ((bf16[8,1,64,512]{3,2,1,0:T(8,128)(2,1)}), bf16[8,1,64,512]{3,2,1,0:T(8,128)(2,1)}, u32[]{:S(2)}, u32[]{:S(2)}) async-start(bf16[8,1,64,512]{3,2,1,0:T(8,128)(2,1)} %bitcast.164), calls=%async_computation.5 | async-start | bytes 1048576 | tf_op jit(solution)/shard_map/all_to_all | solution.py:42
  185.9 8.9 %psum.7 = f32[128]{0:T(128)S(1)} all-reduce(f32[128]{0:T(128)S(1)} %get-tuple-element.2), channel_id=1, replica_groups=mesh['ep'=8,'tp'=4] {'tp'}, use_global_device_ids=true, to_apply=%region_2.3 | all-reduce | flops 128 | bytes 1024 | tf_op jit(solution)/shard_map/psum | solution.py:76
  195.0 10.2 %all_gather.6 = bf16[128,1024]{1,0:T(8,128)(2,1)S(1)} all-gather(bf16[128,256]{1,0:T(8,128)(2,1)S(1)} %multiply_convert_fusion), channel_id=1, replica_groups=mesh['ep'=8,'tp'=4] {'tp'}, dimensions={1}, use_global_device_ids=true | all-gather | bytes 327680 | tf_op jit(solution)/shard_map/all_gather | solution.py:86
  205.1 2.2 convolution_convert_fusion.2
  207.3 1.3 pad_maximum_fusion
  208.6 2.6 %gather_fusion.1 = bf16[512,512]{1,0:T(8,128)(2,1)} fusion(bf16[1024,512]{1,0:T(8,128)(2,1)S(1)} %bitcast.162, s32[1024]{0:T(1024)S(1)} %pad_clamp_fusion), kind=kCustom, calls=%fused_computation.1 | custom fusion | bytes 1050624 | tf_op jit(solution)/shard_map/gather | solution.py:115
  211.3 1.4 reshape.175
  212.6 0.7 multiply_reduce_fusion
  213.4 2.9 %fusion.67 = bf16[128,512]{1,0:T(8,128)(2,1)} fusion(f32[128,512]{1,0:T(8,128)S(1)} %multiply_reduce_fusion, bf16[128,2048]{1,0:T(8,128)(2,1)} %all_gather.7, bf16[2048,512]{1,0:T(8,128)(2,1)} %param.31), kind=kOutput, calls=%fused_computation.38 | convolution fusion | flops 268566528 | bytes 3014656 | tf_op jit(solution)/shard_map/dot_general | solution.py:90
  (52 shorter events, 1.9 us)
Async XLA Ops:
  7.2 83.0 %copy-start = (bf16[1,512,2048]{2,1,0:T(8,128)(2,1)S(1)}, bf16[1,512,2048]{2,1,0:T(8,128)(2,1)}, u32[]{:S(2)}) copy-start(bf16[1,512,2048]{2,1,0:T(8,128)(2,1)} %param.28) | copy-start | bytes 6291460
  81.2 53.4 %all-to-all-start.2 = ((bf16[8,1,64,2048]{3,2,1,0:T(8,128)(2,1)}), bf16[8,1,64,2048]{3,2,1,0:T(8,128)(2,1)}, u32[]{:S(2)}, u32[]{:S(2)}) async-start(bf16[8,1,64,2048]{3,2,1,0:T(8,128)(2,1)} %get-tuple-element.5), calls=%async_computation.3 | async-start | bytes 4194304 | tf_op jit(solution)/shard_map/all_to_all | solution.py:36
  85.5 64.2 %reduce-scatter.3.cloned.1.call-start = ((), (), s32[]{:S(2)}) async-start(), calls=%async_computation.6 | async-start | bytes 2621440 | tf_op jit(solution)/shard_map/reduce_scatter | solution.py:41
  96.4 84.5 %reduce-scatter.5.cloned.1.call-start = ((), (), s32[]{:S(2)}) async-start(), calls=%async_computation.7 | async-start | bytes 2621440 | tf_op jit(solution)/shard_map/reduce_scatter | solution.py:41
  145.3 1.0 copy-start.2
  145.3 1.2 copy-start.7
  145.3 4.3 %copy-start.3 = (f32[128,4]{0,1:T(4,128)S(1)}, f32[128,4]{0,1:T(4,128)}, u32[]{:S(2)}) copy-start(f32[128,4]{0,1:T(4,128)} %param.25) | copy-start | bytes 6148
  148.1 21.6 %collective-permute-start = (bf16[15,256]{1,0:T(8,128)(2,1)S(1)}, bf16[15,256]{1,0:T(8,128)(2,1)S(1)}, u32[]{:S(2)}, u32[]{:S(2)}) collective-permute-start(bf16[15,256]{1,0:T(8,128)(2,1)S(1)} %slice.89), channel_id=1, source_target_pairs={{0,4},{4,8},{8,12},{12,16},{16,20},{20,24},{24,28},{1,5},{5,9},{9,... | collective-permute-start | bytes 23048 | tf_op jit(solution)/shard_map/ppermute | solution.py:14
  149.7 31.2 %all-to-all-start.1 = ((bf16[8,1,64,512]{3,2,1,0:T(8,128)(2,1)}), bf16[8,1,64,512]{3,2,1,0:T(8,128)(2,1)S(1)}, u32[]{:S(2)}, u32[]{:S(2)}) async-start(bf16[8,1,64,512]{3,2,1,0:T(8,128)(2,1)} %bitcast.165), calls=%async_computation.2 | async-start | bytes 1048576 | tf_op jit(solution)/shard_map/all_to_all | solution.py:42
  153.2 2.2 copy-start.6
  155.5 30.1 %copy-start.4 = (f32[256]{0:T(256)S(1)}, f32[256]{0:T(256)}, u32[]{:S(2)}) copy-start(f32[256]{0:T(256)} %param.21) | copy-start | bytes 3076
  156.0 38.9 %copy-start.5 = (f32[256]{0:T(256)S(1)}, f32[256]{0:T(256)}, u32[]{:S(2)}) copy-start(f32[256]{0:T(256)} %param.22) | copy-start | bytes 3076
  181.0 26.4 %copy-start.1 = (bf16[8,1,64,512]{3,2,1,0:T(8,128)(2,1)}, bf16[8,1,64,512]{3,2,1,0:T(8,128)(2,1)S(1)}, u32[]{:S(2)}) copy-start(bf16[8,1,64,512]{3,2,1,0:T(8,128)(2,1)S(1)} %all-to-all-done.1) | copy-start | bytes 1572868
  181.0 26.4 %all-to-all-start.3 = ((bf16[8,1,64,512]{3,2,1,0:T(8,128)(2,1)}), bf16[8,1,64,512]{3,2,1,0:T(8,128)(2,1)}, u32[]{:S(2)}, u32[]{:S(2)}) async-start(bf16[8,1,64,512]{3,2,1,0:T(8,128)(2,1)} %bitcast.164), calls=%async_computation.5 | async-start | bytes 1048576 | tf_op jit(solution)/shard_map/all_to_all | solution.py:42
Sparse Core Ops, SparseCore 0:
  96.6 36.4 reduce-scatter.2
  145.5 35.4 reduce-scatter.4
where the time goes:
time: 224 us; the launch traced here: 223 us
  blocking collectives  88 us (39%)
  waiting for transfers between devices  49.4 us (22%)
  matrix products  30.8 us (14%)
  local copies, waits for them, and re-layouts  19.4 us (9%)
  between operations  14.3 us (6%)
  starting transfers between devices  14 us (6%)
  other arithmetic  7.18 us (3%)
    all_to_all x1, blocking collectives, serve(): lax.all_to_all(sending, 'ep', split_axis=0, concat_axis=0, tiled=True)  55.3 us
    all_to_all x1, waiting for transfers between devices, serve(): lax.all_to_all(sending, 'ep', split_axis=0, concat_axis=0, tiled=True)  38.1 us
    all_gather x1, blocking collectives, on_device(): lax.all_gather(shared_hidden, 'tp', axis=1, tiled=True)  13.6 us
    dot_general x2, matrix products, serve(): jnp.einsum('senf,efd->send', hidden, expert_down, preferred_element_type=...  12.5 us
    reduce_scatter x2, waiting for transfers between devices, serve(): lax.psum_scatter(term.astype(jnp.bfloat16), 'tp', scatter_dimension=3, ti...  11.3 us
    all_gather x1, blocking collectives, on_device(): lax.all_gather(pooled_norm, 'tp', axis=1, tiled=True)  10.2 us
    dot_general x2, matrix products, serve(): jnp.einsum('send,edf->senf', arrived, expert_gate, preferred_element_type...  9.03 us
    psum x1, blocking collectives, on_device(): squares = lax.psum(jnp.sum(scaled * scaled, axis=1), 'tp')  8.92 us
  transfers between devices with their start and end apart: 6, of which 2 were waited for; matrix products, arithmetic and copies ran while one was open for 13% of the time, Pallas kernels for 0%

commit v1 on v0

v1 whole, which is shorter than its diff:
```python
import functools

import jax
import jax.numpy as jnp
from jax import lax
from jax.experimental import pallas as pl
from jax.experimental.pallas import tpu as pltpu
from jax.sharding import PartitionSpec as P

epsilon = 1e-06
reach_rows = 15
window_widths = (2, 4, 8, 16)
CORES = 2
GROUPS = 3
AXES = ("ep", "tp")
VMEM = pl.BlockSpec(memory_space=pltpu.VMEM)


def side_of(size):
    side = 1
    while side * side < size:
        side *= 2
    assert side * side == size
    return side


def routes(n_ep, n_tp, move):
    side = side_of(n_tp)
    pairs = []
    for ep in range(n_ep):
        for tp in range(n_tp):
            z, core, y, x = move(ep // CORES, ep % CORES, tp // side, tp % side)
            pairs.append((ep * n_tp + tp, (z * CORES + core) * n_tp + y * side + x))
    return pairs


def sent(value, n_ep, n_tp, move):
    return lax.ppermute(value, AXES, routes(n_ep, n_tp, move))


def along_z(distance):
    return lambda z, c, y, x: (z ^ distance, c, y, x)


def other_core(z, c, y, x):
    return (z, 1 - c, y, x)


def first_axis(step):
    return lambda z, c, y, x: (z, c, y, x ^ step) if c == 0 else (z, c, y ^ step, x)


def second_axis(step):
    return lambda z, c, y, x: (z, c, y ^ step, x) if c == 0 else (z, c, y, x ^ step)


def column_at(first, second, side):
    core = lax.rem(lax.axis_index("ep"), CORES)
    other = jnp.where(core == 0, second * side + first, first * side + second)
    return lax.bitwise_xor(lax.axis_index("tp"), other.astype(jnp.int32))


def gathered(block, n_ep, n_tp):
    side = side_of(n_tp)
    near = [block] + [sent(block, n_ep, n_tp, first_axis(u)) for u in range(1, side)]
    packed = jnp.concatenate(near, axis=0)
    return near + [sent(packed, n_ep, n_tp, second_axis(u)) for u in range(1, side)]


def silu(value):
    return value / (1.0 + jnp.exp(-value))


def row_norm(rows, gain):
    values = rows.astype(jnp.float32)
    scale = lax.rsqrt(jnp.mean(values * values, axis=-1, keepdims=True) + epsilon)
    return (values * scale * gain).astype(jnp.bfloat16)


def window_means(extended, position, group, n_rows):
    total = jnp.zeros((n_rows, extended.shape[1]), jnp.float32)
    result = jnp.zeros((n_rows, extended.shape[1]), jnp.float32)
    for lag in range(16):
        total = total + extended[reach_rows - lag : reach_rows - lag + n_rows]
        for index, width in enumerate(window_widths):
            if lag + 1 == width:
                count = jnp.minimum(position, float(width))[:, None]
                result = jnp.where(group[None, :] == index, total / count, result)
    return result - extended[reach_rows:]


def norm_kernel(experts, part, x_ref, gain_ref, route_ref, score_ref, all_ref, part_ref):
    width = x_ref.shape[1]

    def rows_of(rows):
        x = x_ref[rows, :].astype(jnp.float32)
        scale = lax.rsqrt(jnp.mean(x * x, axis=1, keepdims=True) + epsilon)
        score = score_ref[rows, :]
        share = 2.5 * score / jnp.sum(score, axis=1, keepdims=True)
        chosen = route_ref[rows, :]
        lanes = lax.broadcasted_iota(jnp.int32, (x.shape[0], all_ref.shape[1] - width), 1)
        expert = jnp.where(lanes < experts, lanes, lanes - experts)
        weight = jnp.zeros(lanes.shape, jnp.float32)
        for k in range(score.shape[1]):
            weight = weight + jnp.where(chosen[:, k : k + 1] == expert, share[:, k : k + 1], 0.0)
        high = weight.astype(jnp.bfloat16)
        low = (weight - high.astype(jnp.float32)).astype(jnp.bfloat16)
        return (x * scale * gain_ref[...]).astype(jnp.bfloat16), jnp.where(
            lanes < experts, high, low
        )

    for target, rows in (
        (part_ref, pl.ds(pl.multiple_of(lax.axis_index("tp") * part, part), part)),
        (all_ref, slice(None)),
    ):
        values, weights = rows_of(rows)
        target[:, :width] = values
        target[:, width:] = weights


def normalized(x, gain, route, score, experts, part):
    lanes = -(-2 * experts // 128) * 128
    shapes = (
        jax.ShapeDtypeStruct((x.shape[0], x.shape[1] + lanes), jnp.bfloat16),
        jax.ShapeDtypeStruct((part, x.shape[1] + lanes), jnp.bfloat16),
    )
    return pl.pallas_call(
        functools.partial(norm_kernel, experts, part),
        out_shape=shapes,
        in_specs=[VMEM] * 4,
        out_specs=(VMEM, VMEM),
        name="row_norm",
    )(x, gain[None, :], route, score)


def expert_kernel(n_pieces, blocks, side, experts, *refs):
    pieces, weights = refs[:n_pieces], refs[n_pieces : n_pieces + 6]
    outs = refs[n_pieces + 6 : n_pieces + 6 + side]
    rows_ref = refs[n_pieces + 6 + side]
    width = weights[0].shape[1]
    n_cols = side * side
    if n_pieces == 1:
        source = pieces[0]
    else:
        source = rows_ref
        part = pieces[0].shape[0] // blocks
        for index, ref in enumerate(pieces):
            for slab in range(ref.shape[0] // (part * blocks)):
                first, second = (index, 0) if index < side else (slab, index - side + 1)
                place = column_at(first, second, side) * part
                for block in range(blocks):
                    start = pl.multiple_of(place + block * part * n_cols, part)
                    at = (slab * blocks + block) * part
                    rows_ref[pl.ds(start, part), :] = ref[at : at + part, :]
    x = source[:, :width]
    extra = source[:, width:].astype(jnp.float32)
    lanes = lax.broadcasted_iota(jnp.int32, extra.shape, 1)
    ep = lax.axis_index("ep")
    hidden = []
    local = weights[0].shape[0]
    for half in range(2):
        gate_ref, up_ref, _ = weights[3 * half : 3 * half + 3]
        owner = ep if half == 0 else lax.bitwise_xor(ep, 1)
        for one in range(local):
            name = owner * local + one
            mine = (lanes == name) | (lanes == name + experts)
            weight = jnp.sum(jnp.where(mine, extra, 0.0), axis=1, keepdims=True)
            gate = jnp.dot(x, gate_ref[one], preferred_element_type=jnp.float32)
            upper = jnp.dot(x, up_ref[one], preferred_element_type=jnp.float32)
            hidden.append((silu(gate) * upper * weight).astype(jnp.bfloat16))
    span = weights[2].shape[2] // n_cols
    for first in range(side):
        for second in range(side):
            start = pl.multiple_of(column_at(first, second, side) * span, span)
            total = jnp.zeros((x.shape[0], span), jnp.float32)
            for half in range(2):
                down_ref = weights[3 * half + 2]
                for one in range(local):
                    total = total + jnp.dot(
                        hidden[half * local + one],
                        down_ref[one, :, pl.ds(start, span)],
                        preferred_element_type=jnp.float32,
                    )
            at = second * span
            outs[first][:, at : at + span] = total.astype(outs[first].dtype)


def expert_partials(pieces, weights, blocks, side, experts, index):
    rows = sum(piece.shape[0] for piece in pieces)
    width = weights[2].shape[2] // side
    shapes = [
        jax.ShapeDtypeStruct((rows, width), jnp.float32 if u == 0 else jnp.bfloat16)
        for u in range(side)
    ]
    whole_rows = 16 if len(pieces) == 1 else rows
    return pl.pallas_call(
        functools.partial(expert_kernel, len(pieces), blocks, side, experts),
        out_shape=shapes,
        in_specs=[VMEM] * (len(pieces) + 6),
        out_specs=[VMEM] * side,
        scratch_shapes=[pltpu.VMEM((whole_rows, pieces[0].shape[1]), jnp.bfloat16)],
        name=f"experts_{index}",
        compiler_params=pltpu.CompilerParams(vmem_limit_bytes=40 << 20),
    )(*pieces, *weights)


def outputs_kernel(side, shared_width, channels, pool_width, *refs):
    n_pieces = 2 * side - 1
    pieces = refs[:n_pieces]
    down_ref, pool_ref, mix_ref, shared_ref = refs[n_pieces:]
    rows = mix_ref.shape[0]
    mix = jnp.zeros(mix_ref.shape, jnp.float32)
    shared = jnp.zeros(shared_ref.shape, jnp.float32)
    squares = jnp.zeros((rows, 1), jnp.float32)
    tail = shared_width + -(-channels // 128) * 128
    for index, ref in enumerate(pieces):
        for slab in range(ref.shape[0] // rows):
            first, second = (index, 0) if index < side else (slab, index - side + 1)
            column = column_at(first, second, side)
            block = slice(slab * rows, (slab + 1) * rows)
            at = pl.ds(pl.multiple_of(column * shared_width, shared_width), shared_width)
            shared = shared + jnp.dot(
                ref[block, :shared_width], down_ref[at, :], preferred_element_type=jnp.float32
            )
            at = pl.ds(pl.multiple_of(column * channels, channels), channels)
            mix = mix + jnp.dot(
                ref[block, shared_width : shared_width + channels],
                pool_ref[at, :],
                preferred_element_type=jnp.float32,
            )
            squares = squares + jnp.sum(
                ref[block, tail:].astype(jnp.float32), axis=1, keepdims=True
            )
    scale = lax.rsqrt(squares / pool_width + epsilon)
    mix_ref[...] = (mix * scale).astype(mix_ref.dtype)
    shared_ref[...] = shared


def outputs(pieces, shared_down, pool_out, side, shared_width, channels):
    rows, span = pieces[0].shape[0], pool_out.shape[1]
    return pl.pallas_call(
        functools.partial(outputs_kernel, side, shared_width, channels, pool_out.shape[0]),
        out_shape=(
            jax.ShapeDtypeStruct((rows, span), jnp.bfloat16),
            jax.ShapeDtypeStruct((rows, span), jnp.float32),
        ),
        in_specs=[VMEM] * (len(pieces) + 2),
        out_specs=(VMEM, VMEM),
        name="outputs",
    )(*pieces, shared_down, pool_out)


def on_device(
    mix_input,
    expert_input,
    mix_gain,
    moe_gain,
    pool_in,
    pool_scale,
    pool_gain,
    pool_out,
    route,
    route_score,
    expert_gate,
    expert_up,
    expert_down,
    shared_gate,
    shared_up,
    shared_down,
):
    n_ep, n_tp = lax.axis_size("ep"), lax.axis_size("tp")
    side, n_z = side_of(n_tp), n_ep // CORES
    tok_rows, channels = mix_input.shape[0], pool_in.shape[1]
    experts = expert_gate.shape[0] * n_ep
    width = pool_out.shape[1]
    send = functools.partial(sent, n_ep=n_ep, n_tp=n_tp)

    all_rows, part_rows = normalized(
        expert_input, moe_gain, route, route_score, experts, tok_rows // n_tp
    )
    from_z = {d: send(part_rows, move=along_z(d)) for d in range(1, n_z)}
    own = (expert_gate, expert_up, expert_down)
    weights = own + tuple(send(w, move=other_core) for w in own)

    mix_norm = row_norm(mix_input, mix_gain)
    pool_input = jnp.dot(mix_norm, pool_in, preferred_element_type=jnp.float32).astype(jnp.bfloat16)
    ahead = [(i * n_tp + j, (i + 1) * n_tp + j) for i in range(n_ep - 1) for j in range(n_tp)]
    before = lax.ppermute(pool_input[tok_rows - reach_rows :], AXES, ahead)
    extended = jnp.concatenate([before, pool_input], axis=0).astype(jnp.float32)
    position = (lax.axis_index("ep") * tok_rows + jnp.arange(tok_rows, dtype=jnp.int32) + 1).astype(
        jnp.float32
    )
    channel_ids = lax.axis_index("tp") * channels + jnp.arange(channels, dtype=jnp.int32)
    group = channel_ids // (channels * n_tp // 4)
    scaled = window_means(extended, position, group, tok_rows) * pool_scale
    squares = jnp.sum(scaled * scaled, axis=1, keepdims=True)
    high = squares.astype(jnp.bfloat16)
    low = (squares - high.astype(jnp.float32)).astype(jnp.bfloat16)
    model_width = expert_input.shape[1]
    shared_hidden = (
        silu(jnp.dot(all_rows[:, :model_width], shared_gate, preferred_element_type=jnp.float32))
        * jnp.dot(all_rows[:, :model_width], shared_up, preferred_element_type=jnp.float32)
    ).astype(jnp.bfloat16)
    filler = -channels % 128
    payload = jnp.concatenate(
        [
            shared_hidden,
            jnp.pad((scaled * pool_gain).astype(jnp.bfloat16), ((0, 0), (0, filler))),
            jnp.pad(jnp.concatenate([high, low], axis=1), ((0, 0), (0, 126))),
        ],
        axis=1,
    )
    pieces = gathered(payload, n_ep, n_tp)
    mix_out, shared_part = outputs(
        pieces, shared_down, pool_out, side, shared_hidden.shape[1], channels
    )

    far = list(range(1, n_z))
    per = -(-len(far) // GROUPS)
    plans = [[0]] + [far[i : i + per] for i in range(0, len(far), per)]
    moe = shared_part
    for index, plan in enumerate(plans):
        if index == 0:
            blocks = [all_rows]
        else:
            mine = jnp.concatenate([from_z[d] for d in plan], axis=0)
            blocks = gathered(mine, n_ep, n_tp)
        outs = expert_partials(blocks, weights, len(plan), side, experts, index)
        total = outs[0]
        for u in range(1, side):
            total = total + send(outs[u], move=first_axis(u)).astype(jnp.float32)
        result = total[:, :width]
        for u in range(1, side):
            piece = total[:, u * width : (u + 1) * width].astype(jnp.bfloat16)
            result = result + send(piece, move=second_axis(u)).astype(jnp.float32)
        if index == 0:
            moe = moe + result
        else:
            result = result.astype(jnp.bfloat16)
            for place, d in enumerate(plan):
                block = result[place * tok_rows : (place + 1) * tok_rows]
                moe = moe + send(block, move=along_z(d)).astype(jnp.float32)
    return (mix_out, moe.astype(jnp.bfloat16))


def solution(mesh):
    return jax.shard_map(
        on_device,
        mesh=mesh,
        in_specs=(
            P("ep", None),
            P("ep", None),
            P(),
            P(),
            P(None, "tp"),
            P("tp"),
            P("tp"),
            P(None, "tp"),
            P("ep", None),
            P("ep", None),
            P("ep", None, "tp"),
            P("ep", None, "tp"),
            P("ep", "tp", None),
            P(None, "tp"),
            P(None, "tp"),
            P(None, "tp"),
        ),
        out_specs=(P("ep", "tp"), P("ep", "tp")),
        check_vma=False,
    )
```

time: 224 us -> 97.9 us (0.44)
  blocking collectives: 88 us -> 0 us
  Pallas kernels: 0 us -> 32.3 us
  waiting for transfers between devices: 49.4 us -> 17.6 us
  matrix products: 30.8 us -> 2.64 us
  starting transfers between devices: 14 us -> 35.2 us
  local copies, waits for them, and re-layouts: 19.4 us -> 4.36 us
  between operations: 14.3 us -> 0.99 us
  other arithmetic: 7.18 us -> 4.45 us
    all_to_all x1 -> x0, blocking collectives: 55.3 us -> none  [serve(): lax.all_to_all(sending, 'ep', split_axis=0, concat_axis=0, tiled=True)]
    all_to_all x3 -> x0, waiting for transfers between devices: 38.1 us -> none  [the longest x1 38.1 us: serve(): lax.all_to_all(sending, 'ep', split_axis=0, concat_axis=0, tiled=True)]
    ppermute x1 -> x26, starting transfers between devices: 1.45 us -> 35.2 us  [the longest x25 33.8 us: sent(): return lax.ppermute(value, AXES, routes(n_ep, n_tp, move))]
    pallas_call x0 -> x6, Pallas kernels: none -> 32.3 us  [the longest x4 26.4 us: expert_partials(): pl.pallas_call(functools.partial(expert_kernel, len(pieces), blocks, side...]
    dot_general x8 -> x2, matrix products: 29.3 us -> 0.88 us  [the longest x1 0.44 us: on_device(): jnp.dot(all_rows[:, :model_width], shared_up, preferred_element_type=jnp....]
    all_gather x2 -> x0, blocking collectives: 23.8 us -> none  [the longest x1 13.6 us: on_device(): lax.all_gather(shared_hidden, 'tp', axis=1, tiled=True)]
    ppermute x1 -> x26, waiting for transfers between devices: 0.01 us -> 17.6 us  [the longest x25 17.6 us: sent(): return lax.ppermute(value, AXES, routes(n_ep, n_tp, move))]
    all_to_all x3 -> x0, starting transfers between devices: 12.5 us -> none  [the longest x2 8.12 us: serve(): return lax.all_to_all(summed, 'ep', split_axis=0, concat_axis=0, tiled=True)]
  transfers between devices with their start and end apart: 6 -> 26, of which waited for: 2 -> 7; matrix products, arithmetic and copies ran while one was open for 13% -> 6% of each run, Pallas kernels for 0% -> 31%
where the time goes in v1:
time: 97.9 us; the launch traced here: 97.6 us
  starting transfers between devices  35.2 us (36%)
  Pallas kernels  32.3 us (33%)
  waiting for transfers between devices  17.6 us (18%)
  other arithmetic  4.45 us (5%)
  local copies, waits for them, and re-layouts  4.36 us (4%)
  matrix products  2.64 us (3%)
  between operations  0.99 us (1%)
    ppermute x25, starting transfers between devices, sent(): return lax.ppermute(value, AXES, routes(n_ep, n_tp, move))  33.8 us
    pallas_call x4, Pallas kernels, expert_partials(): pl.pallas_call(functools.partial(expert_kernel, len(pieces), blocks, side...  26.4 us
    ppermute x25, waiting for transfers between devices, sent(): return lax.ppermute(value, AXES, routes(n_ep, n_tp, move))  17.6 us
    unnamed x20, local copies, waits for them, and re-layouts  4.12 us
    pallas_call x1, Pallas kernels, outputs(): pl.pallas_call(functools.partial(outputs_kernel, side, shared_width, chan...  3.48 us
    pallas_call x1, Pallas kernels, normalized(): pl.pallas_call(functools.partial(norm_kernel, experts, part), out_shape=s...  2.41 us
  transfers between devices with their start and end apart: 26, of which 7 were waited for; matrix products, arithmetic and copies ran while one was open for 6% of the time, Pallas kernels for 31%

profile of v1, /device:TPU:0, one launch (start us, length us, event | category | flops | bytes accessed | tf_op | source)
XLA Modules:
  0.0 97.6 jit_solution(6412794496995380611)
XLA Ops:
  0.6 1.6 %copy.22.route_ref = s32[128,4]{1,0:T(8,128)} copy(s32[128,4]{0,1:T(4,128)} %param.24) | data formatting | bytes 4096 | tf_op args[8]
  2.2 1.4 %copy.23.score_ref = f32[128,4]{1,0:T(8,128)} copy(f32[128,4]{0,1:T(4,128)} %param.25) | data formatting | bytes 4096 | tf_op args[9]
  3.6 2.4 %row_norm.1 = (bf16[128,2176]{1,0:T(8,128)(2,1)}, bf16[32,2176]{1,0:T(8,128)(2,1)}) custom-call(bf16[128,2048]{1,0:T(8,128)(2,1)} %x_ref.1, f32[1,2048]{1,0:T(1,128)} %bitcast.11, s32[128,4]{1,0:T(8,128)} %copy.22.route_ref, f32[128,4]{1,0:T(8,128)} %copy.23.score_ref), custom_call_target="tpu_custom_call" | custom-call | tf_op jit(solution)/shard_map/row_norm/pallas_call | solution.py:127
  6.0 5.1 %collective-permute-start.20 = (bf16[32,2176]{1,0:T(8,128)(2,1)}, bf16[32,2176]{1,0:T(8,128)(2,1)S(1)}, u32[]{:S(2)}, u32[]{:S(2)}) collective-permute-start(bf16[32,2176]{1,0:T(8,128)(2,1)} %get-tuple-element.19), channel_id=1, source_target_pairs={{0,24},{1,25},{2,26},{3,27},{4,28},{5,29},{6,30},{7,31},{8,16},{9,... | collective-permute-start | bytes 417800 | tf_op jit(solution)/shard_map/ppermute | solution.py:38
  11.1 1.2 %fusion.1 = f32[128]{0:T(128)S(1)} fusion(bf16[128,2048]{1,0:T(8,128)(2,1)} %param.16), kind=kLoop, calls=%fused_computation.5 | loop fusion | flops 786304 | bytes 524800 | tf_op jit(solution)/shard_map/reduce_sum | solution.py:76
  12.4 1.8 %convolution_convert_fusion = bf16[128,256]{1,0:T(8,128)(2,1)S(1)} fusion(bf16[2048,256]{1,0:T(8,128)(2,1)} %param.20, bf16[128,2048]{1,0:T(8,128)(2,1)} %param.16, f32[2048]{0:T(1024)} %param.18, f32[128]{0:T(128)S(1)} %add_rsqrt_fusion), kind=kOutput, calls=%fused_computation.4 | convolution fusion | flops 135299072 | bytes 1647104 | tf_op jit(solution)/shard_map/dot_general | solution.py:286
  14.1 1.5 %collective-permute-start = (bf16[15,256]{1,0:T(8,128)(2,1)S(1)}, bf16[15,256]{1,0:T(8,128)(2,1)S(1)}, u32[]{:S(2)}, u32[]{:S(2)}) collective-permute-start(bf16[15,256]{1,0:T(8,128)(2,1)S(1)} %slice.110), channel_id=1, source_target_pairs={{0,4},{1,5},{2,6},{3,7},{4,8},{5,9},{6,10},{7,11},{8,12},{9,13},{1... | collective-permute-start | bytes 23048 | tf_op jit(solution)/shard_map/ppermute | solution.py:288
  15.6 1.3 %collective-permute-start.3 = (bf16[1,2048,512]{2,1,0:T(8,128)(2,1)}, bf16[1,2048,512]{2,1,0:T(8,128)(2,1)}, u32[]{:S(2)}, u32[]{:S(2)}) collective-permute-start(bf16[1,2048,512]{2,1,0:T(8,128)(2,1)} %refs_3_.9), channel_id=1, source_target_pairs={{0,4},{1,5},{2,6},{3,7},{4,0},{5,1},{6,2},{7,3},{8,12},{9,13},{10,... | collective-permute-start | bytes 6291464 | tf_op jit(solution)/shard_map/ppermute | solution.py:38
  20.0 2.9 %collective-permute-start.8 = (bf16[32,2176]{1,0:T(8,128)(2,1)}, bf16[32,2176]{1,0:T(8,128)(2,1)S(1)}, u32[]{:S(2)}, u32[]{:S(2)}) collective-permute-start(bf16[32,2176]{1,0:T(8,128)(2,1)} %get-tuple-element.19), channel_id=1, source_target_pairs={{0,8},{1,9},{2,10},{3,11},{4,12},{5,13},{6,14},{7,15},{8,0},{9,1},... | collective-permute-start | bytes 417800 | tf_op jit(solution)/shard_map/ppermute | solution.py:38
  23.1 1.5 %collective-permute-start.21 = (bf16[32,2176]{1,0:T(8,128)(2,1)S(1)}, bf16[32,2176]{1,0:T(8,128)(2,1)S(1)}, u32[]{:S(2)}, u32[]{:S(2)}) collective-permute-start(bf16[32,2176]{1,0:T(8,128)(2,1)S(1)} %collective-permute-done.20.refs_0_), channel_id=1, source_target_pairs={{0,1},{1,0},{2,3},{3,2},{4,6},{5,7},{6,4},{7,5},{8,9},{9,8},{10,11... | collective-permute-start | bytes 417800 | tf_op jit(solution)/shard_map/ppermute | solution.py:38
  24.8 2.2 %collective-permute-done.8.refs_0_ = bf16[32,2176]{1,0:T(8,128)(2,1)S(1)} collective-permute-done((bf16[32,2176]{1,0:T(8,128)(2,1)}, bf16[32,2176]{1,0:T(8,128)(2,1)S(1)}, u32[]{:S(2)}, u32[]{:S(2)}) %collective-permute-start.8) | collective-permute-done | bytes 139296 | tf_op jit(solution)/shard_map/ppermute | solution.py:38
  27.1 1.5 %collective-permute-start.15 = (bf16[32,2176]{1,0:T(8,128)(2,1)S(1)}, bf16[32,2176]{1,0:T(8,128)(2,1)S(1)}, u32[]{:S(2)}, u32[]{:S(2)}) collective-permute-start(bf16[32,2176]{1,0:T(8,128)(2,1)S(1)} %collective-permute-done.14.refs_0_), channel_id=1, source_target_pairs={{0,1},{1,0},{2,3},{3,2},{4,6},{5,7},{6,4},{7,5},{8,9},{9,8},{10,11... | collective-permute-start | bytes 417800 | tf_op jit(solution)/shard_map/ppermute | solution.py:38
  28.5 1.1 %collective-permute-start.9 = (bf16[32,2176]{1,0:T(8,128)(2,1)S(1)}, bf16[32,2176]{1,0:T(8,128)(2,1)S(1)}, u32[]{:S(2)}, u32[]{:S(2)}) collective-permute-start(bf16[32,2176]{1,0:T(8,128)(2,1)S(1)} %collective-permute-done.8.refs_0_), channel_id=1, source_target_pairs={{0,1},{1,0},{2,3},{3,2},{4,6},{5,7},{6,4},{7,5},{8,9},{9,8},{10,11... | collective-permute-start | bytes 417800 | tf_op jit(solution)/shard_map/ppermute | solution.py:38
  29.7 2.4 %collective-permute-done.15.refs_1_ = bf16[32,2176]{1,0:T(8,128)(2,1)S(1)} collective-permute-done((bf16[32,2176]{1,0:T(8,128)(2,1)S(1)}, bf16[32,2176]{1,0:T(8,128)(2,1)S(1)}, u32[]{:S(2)}, u32[]{:S(2)}) %collective-permute-start.15) | collective-permute-done | bytes 139296 | tf_op jit(solution)/shard_map/ppermute | solution.py:38
  32.1 1.5 %collective-permute-start.22 = (bf16[64,2176]{1,0:T(8,128)(2,1)S(1)}, bf16[64,2176]{1,0:T(8,128)(2,1)S(1)}, u32[]{:S(2)}, u32[]{:S(2)}) collective-permute-start(bf16[64,2176]{1,0:T(8,128)(2,1)S(1)} %pad_maximum_fusion.3), channel_id=1, source_target_pairs={{0,2},{1,3},{2,0},{3,1},{4,5},{5,4},{6,7},{7,6},{8,10},{9,11},{10,... | collective-permute-start | bytes 835592 | tf_op jit(solution)/shard_map/ppermute | solution.py:38
  33.8 1.5 %collective-permute-start.1 = (bf16[128,896]{1,0:T(8,128)(2,1)S(1)}, bf16[128,896]{1,0:T(8,128)(2,1)S(1)}, u32[]{:S(2)}, u32[]{:S(2)}) collective-permute-start(bf16[128,896]{1,0:T(8,128)(2,1)S(1)} %pad_maximum_fusion.4.refs_0_), channel_id=1, source_target_pairs={{0,1},{1,0},{2,3},{3,2},{4,6},{5,7},{6,4},{7,5},{8,9},{9,8},{10,11... | collective-permute-start | bytes 688136 | tf_op jit(solution)/shard_map/ppermute | solution.py:38
  35.3 5.0 %collective-permute-done.22.refs_2_ = bf16[64,2176]{1,0:T(8,128)(2,1)S(1)} collective-permute-done((bf16[64,2176]{1,0:T(8,128)(2,1)S(1)}, bf16[64,2176]{1,0:T(8,128)(2,1)S(1)}, u32[]{:S(2)}, u32[]{:S(2)}) %collective-permute-start.22) | collective-permute-done | bytes 278560 | tf_op jit(solution)/shard_map/ppermute | solution.py:38
  40.3 1.5 %collective-permute-start.16 = (bf16[64,2176]{1,0:T(8,128)(2,1)S(1)}, bf16[64,2176]{1,0:T(8,128)(2,1)S(1)}, u32[]{:S(2)}, u32[]{:S(2)}) collective-permute-start(bf16[64,2176]{1,0:T(8,128)(2,1)S(1)} %pad_maximum_fusion.2), channel_id=1, source_target_pairs={{0,2},{1,3},{2,0},{3,1},{4,5},{5,4},{6,7},{7,6},{8,10},{9,11},{10,... | collective-permute-start | bytes 835592 | tf_op jit(solution)/shard_map/ppermute | solution.py:38
  42.4 6.6 %experts_3.1 = (f32[128,1024]{1,0:T(8,128)S(1)}, bf16[128,1024]{1,0:T(8,128)(2,1)S(1)}) custom-call(bf16[32,2176]{1,0:T(8,128)(2,1)S(1)} %collective-permute-done.20.refs_0_, bf16[32,2176]{1,0:T(8,128)(2,1)S(1)} %collective-permute-done.21.refs_1_, bf16[64,2176]{1,0:T(8,128)(2,1)S(1)} %collective-permute-done.22.refs_2_, bf16[1,2048,512]{2,1,0:T(8,128)(2,1)} %refs_3_.9, ...), custom_call_target="tpu_custom_call" | custom-call | tf_op jit(solution)/shard_map/experts_3/pallas_call | solution.py:196
  49.1 1.6 %collective-permute-start.23 = (bf16[128,1024]{1,0:T(8,128)(2,1)S(1)}, bf16[128,1024]{1,0:T(8,128)(2,1)S(1)}, u32[]{:S(2)}, u32[]{:S(2)}) collective-permute-start(bf16[128,1024]{1,0:T(8,128)(2,1)S(1)} %get-tuple-element.25), channel_id=1, source_target_pairs={{0,1},{1,0},{2,3},{3,2},{4,6},{5,7},{6,4},{7,5},{8,9},{9,8},{10,11... | collective-permute-start | bytes 786440 | tf_op jit(solution)/shard_map/ppermute | solution.py:38
  50.6 6.6 %experts_2.1 = (f32[128,1024]{1,0:T(8,128)S(1)}, bf16[128,1024]{1,0:T(8,128)(2,1)S(1)}) custom-call(bf16[32,2176]{1,0:T(8,128)(2,1)S(1)} %collective-permute-done.14.refs_0_, bf16[32,2176]{1,0:T(8,128)(2,1)S(1)} %collective-permute-done.15.refs_1_, bf16[64,2176]{1,0:T(8,128)(2,1)S(1)} %collective-permute-done.16.refs_2_, bf16[1,2048,512]{2,1,0:T(8,128)(2,1)} %refs_3_.9, ...), custom_call_target="tpu_custom_call" | custom-call | tf_op jit(solution)/shard_map/experts_2/pallas_call | solution.py:196
  57.9 1.6 %collective-permute-start.2 = (bf16[256,896]{1,0:T(8,128)(2,1)S(1)}, bf16[256,896]{1,0:T(8,128)(2,1)}, u32[]{:S(2)}, u32[]{:S(2)}) collective-permute-start(bf16[256,896]{1,0:T(8,128)(2,1)S(1)} %pad_maximum_fusion), channel_id=1, source_target_pairs={{0,2},{1,3},{2,0},{3,1},{4,5},{5,4},{6,7},{7,6},{8,10},{9,11},{10,... | collective-permute-start | bytes 1376264 | tf_op jit(solution)/shard_map/ppermute | solution.py:38
  59.5 6.6 %experts_0.1 = (f32[128,1024]{1,0:T(8,128)S(1)}, bf16[128,1024]{1,0:T(8,128)(2,1)S(1)}) custom-call(bf16[128,2176]{1,0:T(8,128)(2,1)S(1)} %copy-done.1, bf16[1,2048,512]{2,1,0:T(8,128)(2,1)} %refs_3_.9, bf16[1,2048,512]{2,1,0:T(8,128)(2,1)} %refs_4_.7, bf16[1,512,2048]{2,1,0:T(8,128)(2,1)} %refs_5_.5, ...), custom_call_target="tpu_custom_call" | custom-call | tf_op jit(solution)/shard_map/experts_0/pallas_call | solution.py:196
  66.1 1.6 %collective-permute-start.6 = (bf16[128,1024]{1,0:T(8,128)(2,1)S(1)}, bf16[128,1024]{1,0:T(8,128)(2,1)S(1)}, u32[]{:S(2)}, u32[]{:S(2)}) collective-permute-start(bf16[128,1024]{1,0:T(8,128)(2,1)S(1)} %get-tuple-element.18), channel_id=1, source_target_pairs={{0,1},{1,0},{2,3},{3,2},{4,6},{5,7},{6,4},{7,5},{8,9},{9,8},{10,11... | collective-permute-start | bytes 786440 | tf_op jit(solution)/shard_map/ppermute | solution.py:38
  67.7 6.6 %experts_1.1 = (f32[128,1024]{1,0:T(8,128)S(1)}, bf16[128,1024]{1,0:T(8,128)(2,1)S(1)}) custom-call(bf16[32,2176]{1,0:T(8,128)(2,1)S(1)} %collective-permute-done.8.refs_0_, bf16[32,2176]{1,0:T(8,128)(2,1)S(1)} %collective-permute-done.9.refs_1_, bf16[64,2176]{1,0:T(8,128)(2,1)S(1)} %collective-permute-done.10.refs_2_, bf16[1,2048,512]{2,1,0:T(8,128)(2,1)} %refs_3_.9, ...), custom_call_target="tpu_custom_call" | custom-call | tf_op jit(solution)/shard_map/experts_1/pallas_call | solution.py:196
  75.7 1.6 %collective-permute-start.18 = (bf16[128,512]{1,0:T(8,128)(2,1)S(1)}, bf16[128,512]{1,0:T(8,128)(2,1)S(1)}, u32[]{:S(2)}, u32[]{:S(2)}) collective-permute-start(bf16[128,512]{1,0:T(8,128)(2,1)S(1)} %slice.224), channel_id=1, source_target_pairs={{0,2},{1,3},{2,0},{3,1},{4,5},{5,4},{6,7},{7,6},{8,10},{9,11},{10,... | collective-permute-start | bytes 393224 | tf_op jit(solution)/shard_map/ppermute | solution.py:38
  77.2 5.4 %collective-permute-done.11 = bf16[128,1024]{1,0:T(8,128)(2,1)S(1)} collective-permute-done((bf16[128,1024]{1,0:T(8,128)(2,1)S(1)}, bf16[128,1024]{1,0:T(8,128)(2,1)S(1)}, u32[]{:S(2)}, u32[]{:S(2)}) %collective-permute-start.11) | collective-permute-done | bytes 262176 | tf_op jit(solution)/shard_map/ppermute | solution.py:38
  83.5 1.6 %collective-permute-start.7 = (bf16[128,512]{1,0:T(8,128)(2,1)S(1)}, bf16[128,512]{1,0:T(8,128)(2,1)S(1)}, u32[]{:S(2)}, u32[]{:S(2)}) collective-permute-start(bf16[128,512]{1,0:T(8,128)(2,1)S(1)} %slice.226), channel_id=1, source_target_pairs={{0,2},{1,3},{2,0},{3,1},{4,5},{5,4},{6,7},{7,6},{8,10},{9,11},{10,... | collective-permute-start | bytes 393224 | tf_op jit(solution)/shard_map/ppermute | solution.py:38
  85.0 3.5 %collective-permute-start.25 = (bf16[128,512]{1,0:T(8,128)(2,1)S(1)}, bf16[128,512]{1,0:T(8,128)(2,1)S(1)}, u32[]{:S(2)}, u32[]{:S(2)}) collective-permute-start(bf16[128,512]{1,0:T(8,128)(2,1)S(1)} %fusion.10), channel_id=1, source_target_pairs={{0,24},{1,25},{2,26},{3,27},{4,28},{5,29},{6,30},{7,31},{8,16},{9,... | collective-permute-start | bytes 393224 | tf_op jit(solution)/shard_map/ppermute | solution.py:38
  90.3 3.5 %outputs.1 = (bf16[128,512]{1,0:T(8,128)(2,1)}, f32[128,512]{1,0:T(8,128)}) custom-call(bf16[128,896]{1,0:T(8,128)(2,1)} %copy-done.3, bf16[128,896]{1,0:T(8,128)(2,1)} %copy-done.2, bf16[256,896]{1,0:T(8,128)(2,1)} %collective-permute-done.2.refs_2_, bf16[2048,512]{1,0:T(8,128)(2,1)} %refs_3_.5, bf16[1024,512]{1,0:T(8,128)(2,1)} %refs_4_.4), custom_call_target="tpu_custom_call" | custom-call | tf_op jit(solution)/shard_map/outputs/pallas_call | solution.py:241
  93.8 2.1 %collective-permute-done.19 = bf16[128,512]{1,0:T(8,128)(2,1)S(1)} collective-permute-done((bf16[128,512]{1,0:T(8,128)(2,1)S(1)}, bf16[128,512]{1,0:T(8,128)(2,1)S(1)}, u32[]{:S(2)}, u32[]{:S(2)}) %collective-permute-start.19) | collective-permute-done | bytes 131104 | tf_op jit(solution)/shard_map/ppermute | solution.py:38
  95.9 1.7 %fusion.17 = bf16[128,512]{1,0:T(8,128)(2,1)} fusion(f32[128,512]{1,0:T(8,128)} %get-tuple-element.16, f32[128,1024]{1,0:T(8,128)S(1)} %convert_add_fusion.3, bf16[128,512]{1,0:T(8,128)(2,1)S(1)} %collective-permute-done.25, bf16[128,512]{1,0:T(8,128)(2,1)S(1)} %collective-permute-done.19, bf16[128,512]{1,0:T(8,128)(2,1)S(1)} %collective-permute-done.13, ...), kind=kLoop, calls=%fused_computation.36 | loop fusion | flops 655360 | bytes 1179648 | tf_op jit(solution)/shard_map/convert_element_type | solution.py:343
  (81 shorter events, 8.8 us)
Async XLA Ops:
  0.6 16.4 %copy-start = (bf16[2048,512]{1,0:T(8,128)(2,1)S(1)}, bf16[2048,512]{1,0:T(8,128)(2,1)}, u32[]{:S(2)}) copy-start(bf16[2048,512]{1,0:T(8,128)(2,1)} %param.29) | copy-start | bytes 6291460
  6.0 11.0 %copy-start.1 = (bf16[128,2176]{1,0:T(8,128)(2,1)S(1)}, bf16[128,2176]{1,0:T(8,128)(2,1)}, u32[]{:S(2)}) copy-start(bf16[128,2176]{1,0:T(8,128)(2,1)} %get-tuple-element.14.refs_0_) | copy-start | bytes 1671172
  6.0 13.9 %collective-permute-start.20 = (bf16[32,2176]{1,0:T(8,128)(2,1)}, bf16[32,2176]{1,0:T(8,128)(2,1)S(1)}, u32[]{:S(2)}, u32[]{:S(2)}) collective-permute-start(bf16[32,2176]{1,0:T(8,128)(2,1)} %get-tuple-element.19), channel_id=1, source_target_pairs={{0,24},{1,25},{2,26},{3,27},{4,28},{5,29},{6,30},{7,31},{8,16},{9,... | collective-permute-start | bytes 417800 | tf_op jit(solution)/shard_map/ppermute | solution.py:38
  11.1 12.0 %collective-permute-start.14 = (bf16[32,2176]{1,0:T(8,128)(2,1)}, bf16[32,2176]{1,0:T(8,128)(2,1)S(1)}, u32[]{:S(2)}, u32[]{:S(2)}) collective-permute-start(bf16[32,2176]{1,0:T(8,128)(2,1)} %get-tuple-element.19), channel_id=1, source_target_pairs={{0,16},{1,17},{2,18},{3,19},{4,20},{5,21},{6,22},{7,23},{8,24},{9,... | collective-permute-start | bytes 417800 | tf_op jit(solution)/shard_map/ppermute | solution.py:38
  14.1 4.9 %collective-permute-start = (bf16[15,256]{1,0:T(8,128)(2,1)S(1)}, bf16[15,256]{1,0:T(8,128)(2,1)S(1)}, u32[]{:S(2)}, u32[]{:S(2)}) collective-permute-start(bf16[15,256]{1,0:T(8,128)(2,1)S(1)} %slice.110), channel_id=1, source_target_pairs={{0,4},{1,5},{2,6},{3,7},{4,8},{5,9},{6,10},{7,11},{8,12},{9,13},{1... | collective-permute-start | bytes 23048 | tf_op jit(solution)/shard_map/ppermute | solution.py:288
  15.6 26.2 %collective-permute-start.3 = (bf16[1,2048,512]{2,1,0:T(8,128)(2,1)}, bf16[1,2048,512]{2,1,0:T(8,128)(2,1)}, u32[]{:S(2)}, u32[]{:S(2)}) collective-permute-start(bf16[1,2048,512]{2,1,0:T(8,128)(2,1)} %refs_3_.9), channel_id=1, source_target_pairs={{0,4},{1,5},{2,6},{3,7},{4,0},{5,1},{6,2},{7,3},{8,12},{9,13},{10,... | collective-permute-start | bytes 6291464 | tf_op jit(solution)/shard_map/ppermute | solution.py:38
  16.9 25.6 %collective-permute-start.4 = (bf16[1,2048,512]{2,1,0:T(8,128)(2,1)}, bf16[1,2048,512]{2,1,0:T(8,128)(2,1)}, u32[]{:S(2)}, u32[]{:S(2)}) collective-permute-start(bf16[1,2048,512]{2,1,0:T(8,128)(2,1)} %refs_4_.7), channel_id=1, source_target_pairs={{0,4},{1,5},{2,6},{3,7},{4,0},{5,1},{6,2},{7,3},{8,12},{9,13},{10,... | collective-permute-start | bytes 6291464 | tf_op jit(solution)/shard_map/ppermute | solution.py:38
  19.0 14.6 %copy-start.4 = (bf16[128,512]{1,0:T(8,128)(2,1)}, bf16[128,512]{1,0:T(8,128)(2,1)S(1)}, u32[]{:S(2)}) copy-start(bf16[128,512]{1,0:T(8,128)(2,1)S(1)} %fusion) | copy-start | bytes 393220
  19.1 23.4 %collective-permute-start.5 = (bf16[1,512,2048]{2,1,0:T(8,128)(2,1)}, bf16[1,512,2048]{2,1,0:T(8,128)(2,1)}, u32[]{:S(2)}, u32[]{:S(2)}) collective-permute-start(bf16[1,512,2048]{2,1,0:T(8,128)(2,1)} %refs_5_.5), channel_id=1, source_target_pairs={{0,4},{1,5},{2,6},{3,7},{4,0},{5,1},{6,2},{7,3},{8,12},{9,13},{10,... | collective-permute-start | bytes 6291464 | tf_op jit(solution)/shard_map/ppermute | solution.py:38
  20.0 7.1 %collective-permute-start.8 = (bf16[32,2176]{1,0:T(8,128)(2,1)}, bf16[32,2176]{1,0:T(8,128)(2,1)S(1)}, u32[]{:S(2)}, u32[]{:S(2)}) collective-permute-start(bf16[32,2176]{1,0:T(8,128)(2,1)} %get-tuple-element.19), channel_id=1, source_target_pairs={{0,8},{1,9},{2,10},{3,11},{4,12},{5,13},{6,14},{7,15},{8,0},{9,1},... | collective-permute-start | bytes 417800 | tf_op jit(solution)/shard_map/ppermute | solution.py:38
  23.1 5.4 %collective-permute-start.21 = (bf16[32,2176]{1,0:T(8,128)(2,1)S(1)}, bf16[32,2176]{1,0:T(8,128)(2,1)S(1)}, u32[]{:S(2)}, u32[]{:S(2)}) collective-permute-start(bf16[32,2176]{1,0:T(8,128)(2,1)S(1)} %collective-permute-done.20.refs_0_), channel_id=1, source_target_pairs={{0,1},{1,0},{2,3},{3,2},{4,6},{5,7},{6,4},{7,5},{8,9},{9,8},{10,11... | collective-permute-start | bytes 417800 | tf_op jit(solution)/shard_map/ppermute | solution.py:38
  24.8 24.3 %copy-start.3 = (bf16[128,896]{1,0:T(8,128)(2,1)}, bf16[128,896]{1,0:T(8,128)(2,1)S(1)}, u32[]{:S(2)}) copy-start(bf16[128,896]{1,0:T(8,128)(2,1)S(1)} %pad_maximum_fusion.4.refs_0_) | copy-start | bytes 688132
  27.1 5.1 %collective-permute-start.15 = (bf16[32,2176]{1,0:T(8,128)(2,1)S(1)}, bf16[32,2176]{1,0:T(8,128)(2,1)S(1)}, u32[]{:S(2)}, u32[]{:S(2)}) collective-permute-start(bf16[32,2176]{1,0:T(8,128)(2,1)S(1)} %collective-permute-done.14.refs_0_), channel_id=1, source_target_pairs={{0,1},{1,0},{2,3},{3,2},{4,6},{5,7},{6,4},{7,5},{8,9},{9,8},{10,11... | collective-permute-start | bytes 417800 | tf_op jit(solution)/shard_map/ppermute | solution.py:38
  28.5 5.3 %collective-permute-start.9 = (bf16[32,2176]{1,0:T(8,128)(2,1)S(1)}, bf16[32,2176]{1,0:T(8,128)(2,1)S(1)}, u32[]{:S(2)}, u32[]{:S(2)}) collective-permute-start(bf16[32,2176]{1,0:T(8,128)(2,1)S(1)} %collective-permute-done.8.refs_0_), channel_id=1, source_target_pairs={{0,1},{1,0},{2,3},{3,2},{4,6},{5,7},{6,4},{7,5},{8,9},{9,8},{10,11... | collective-permute-start | bytes 417800 | tf_op jit(solution)/shard_map/ppermute | solution.py:38
  32.1 8.2 %collective-permute-start.22 = (bf16[64,2176]{1,0:T(8,128)(2,1)S(1)}, bf16[64,2176]{1,0:T(8,128)(2,1)S(1)}, u32[]{:S(2)}, u32[]{:S(2)}) collective-permute-start(bf16[64,2176]{1,0:T(8,128)(2,1)S(1)} %pad_maximum_fusion.3), channel_id=1, source_target_pairs={{0,2},{1,3},{2,0},{3,1},{4,5},{5,4},{6,7},{7,6},{8,10},{9,11},{10,... | collective-permute-start | bytes 835592 | tf_op jit(solution)/shard_map/ppermute | solution.py:38
  33.8 24.0 %collective-permute-start.1 = (bf16[128,896]{1,0:T(8,128)(2,1)S(1)}, bf16[128,896]{1,0:T(8,128)(2,1)S(1)}, u32[]{:S(2)}, u32[]{:S(2)}) collective-permute-start(bf16[128,896]{1,0:T(8,128)(2,1)S(1)} %pad_maximum_fusion.4.refs_0_), channel_id=1, source_target_pairs={{0,1},{1,0},{2,3},{3,2},{4,6},{5,7},{6,4},{7,5},{8,9},{9,8},{10,11... | collective-permute-start | bytes 688136 | tf_op jit(solution)/shard_map/ppermute | solution.py:38
  40.3 10.3 %collective-permute-start.16 = (bf16[64,2176]{1,0:T(8,128)(2,1)S(1)}, bf16[64,2176]{1,0:T(8,128)(2,1)S(1)}, u32[]{:S(2)}, u32[]{:S(2)}) collective-permute-start(bf16[64,2176]{1,0:T(8,128)(2,1)S(1)} %pad_maximum_fusion.2), channel_id=1, source_target_pairs={{0,2},{1,3},{2,0},{3,1},{4,5},{5,4},{6,7},{7,6},{8,10},{9,11},{10,... | collective-permute-start | bytes 835592 | tf_op jit(solution)/shard_map/ppermute | solution.py:38
  41.8 25.8 %collective-permute-start.10 = (bf16[64,2176]{1,0:T(8,128)(2,1)S(1)}, bf16[64,2176]{1,0:T(8,128)(2,1)S(1)}, u32[]{:S(2)}, u32[]{:S(2)}) collective-permute-start(bf16[64,2176]{1,0:T(8,128)(2,1)S(1)} %pad_maximum_fusion.1), channel_id=1, source_target_pairs={{0,2},{1,3},{2,0},{3,1},{4,5},{5,4},{6,7},{7,6},{8,10},{9,11},{10,... | collective-permute-start | bytes 835592 | tf_op jit(solution)/shard_map/ppermute | solution.py:38
  49.1 8.8 %copy-start.5 = (bf16[128,512]{1,0:T(8,128)(2,1)S(1)}, bf16[128,512]{1,0:T(8,128)(2,1)}, u32[]{:S(2)}) copy-start(bf16[128,512]{1,0:T(8,128)(2,1)} %copy-done.4) | copy-start | bytes 393220
  49.1 25.8 %collective-permute-start.23 = (bf16[128,1024]{1,0:T(8,128)(2,1)S(1)}, bf16[128,1024]{1,0:T(8,128)(2,1)S(1)}, u32[]{:S(2)}, u32[]{:S(2)}) collective-permute-start(bf16[128,1024]{1,0:T(8,128)(2,1)S(1)} %get-tuple-element.25), channel_id=1, source_target_pairs={{0,1},{1,0},{2,3},{3,2},{4,6},{5,7},{6,4},{7,5},{8,9},{9,8},{10,11... | collective-permute-start | bytes 786440 | tf_op jit(solution)/shard_map/ppermute | solution.py:38
  57.2 18.3 %collective-permute-start.17 = (bf16[128,1024]{1,0:T(8,128)(2,1)S(1)}, bf16[128,1024]{1,0:T(8,128)(2,1)S(1)}, u32[]{:S(2)}, u32[]{:S(2)}) collective-permute-start(bf16[128,1024]{1,0:T(8,128)(2,1)S(1)} %get-tuple-element.23), channel_id=1, source_target_pairs={{0,1},{1,0},{2,3},{3,2},{4,6},{5,7},{6,4},{7,5},{8,9},{9,8},{10,11... | collective-permute-start | bytes 786440 | tf_op jit(solution)/shard_map/ppermute | solution.py:38
  57.9 8.2 %copy-start.2 = (bf16[128,896]{1,0:T(8,128)(2,1)}, bf16[128,896]{1,0:T(8,128)(2,1)S(1)}, u32[]{:S(2)}) copy-start(bf16[128,896]{1,0:T(8,128)(2,1)S(1)} %collective-permute-done.1.refs_1_) | copy-start | bytes 688132
  57.9 32.4 %collective-permute-start.2 = (bf16[256,896]{1,0:T(8,128)(2,1)S(1)}, bf16[256,896]{1,0:T(8,128)(2,1)}, u32[]{:S(2)}, u32[]{:S(2)}) collective-permute-start(bf16[256,896]{1,0:T(8,128)(2,1)S(1)} %pad_maximum_fusion), channel_id=1, source_target_pairs={{0,2},{1,3},{2,0},{3,1},{4,5},{5,4},{6,7},{7,6},{8,10},{9,11},{10,... | collective-permute-start | bytes 1376264 | tf_op jit(solution)/shard_map/ppermute | solution.py:38
  66.1 17.3 %collective-permute-start.6 = (bf16[128,1024]{1,0:T(8,128)(2,1)S(1)}, bf16[128,1024]{1,0:T(8,128)(2,1)S(1)}, u32[]{:S(2)}, u32[]{:S(2)}) collective-permute-start(bf16[128,1024]{1,0:T(8,128)(2,1)S(1)} %get-tuple-element.18), channel_id=1, source_target_pairs={{0,1},{1,0},{2,3},{3,2},{4,6},{5,7},{6,4},{7,5},{8,9},{9,8},{10,11... | collective-permute-start | bytes 786440 | tf_op jit(solution)/shard_map/ppermute | solution.py:38
  74.3 8.4 %collective-permute-start.11 = (bf16[128,1024]{1,0:T(8,128)(2,1)S(1)}, bf16[128,1024]{1,0:T(8,128)(2,1)S(1)}, u32[]{:S(2)}, u32[]{:S(2)}) collective-permute-start(bf16[128,1024]{1,0:T(8,128)(2,1)S(1)} %get-tuple-element.21), channel_id=1, source_target_pairs={{0,1},{1,0},{2,3},{3,2},{4,6},{5,7},{6,4},{7,5},{8,9},{9,8},{10,11... | collective-permute-start | bytes 786440 | tf_op jit(solution)/shard_map/ppermute | solution.py:38
  75.0 10.0 %collective-permute-start.24 = (bf16[128,512]{1,0:T(8,128)(2,1)S(1)}, bf16[128,512]{1,0:T(8,128)(2,1)S(1)}, u32[]{:S(2)}, u32[]{:S(2)}) collective-permute-start(bf16[128,512]{1,0:T(8,128)(2,1)S(1)} %slice.223), channel_id=1, source_target_pairs={{0,2},{1,3},{2,0},{3,1},{4,5},{5,4},{6,7},{7,6},{8,10},{9,11},{10,... | collective-permute-start | bytes 393224 | tf_op jit(solution)/shard_map/ppermute | solution.py:38
  75.7 12.8 %collective-permute-start.18 = (bf16[128,512]{1,0:T(8,128)(2,1)S(1)}, bf16[128,512]{1,0:T(8,128)(2,1)S(1)}, u32[]{:S(2)}, u32[]{:S(2)}) collective-permute-start(bf16[128,512]{1,0:T(8,128)(2,1)S(1)} %slice.224), channel_id=1, source_target_pairs={{0,2},{1,3},{2,0},{3,1},{4,5},{5,4},{6,7},{7,6},{8,10},{9,11},{10,... | collective-permute-start | bytes 393224 | tf_op jit(solution)/shard_map/ppermute | solution.py:38
  82.8 6.0 %collective-permute-start.12 = (bf16[128,512]{1,0:T(8,128)(2,1)S(1)}, bf16[128,512]{1,0:T(8,128)(2,1)S(1)}, u32[]{:S(2)}, u32[]{:S(2)}) collective-permute-start(bf16[128,512]{1,0:T(8,128)(2,1)S(1)} %slice.225), channel_id=1, source_target_pairs={{0,2},{1,3},{2,0},{3,1},{4,5},{5,4},{6,7},{7,6},{8,10},{9,11},{10,... | collective-permute-start | bytes 393224 | tf_op jit(solution)/shard_map/ppermute | solution.py:38
  83.5 10.3 %collective-permute-start.7 = (bf16[128,512]{1,0:T(8,128)(2,1)S(1)}, bf16[128,512]{1,0:T(8,128)(2,1)S(1)}, u32[]{:S(2)}, u32[]{:S(2)}) collective-permute-start(bf16[128,512]{1,0:T(8,128)(2,1)S(1)} %slice.226), channel_id=1, source_target_pairs={{0,2},{1,3},{2,0},{3,1},{4,5},{5,4},{6,7},{7,6},{8,10},{9,11},{10,... | collective-permute-start | bytes 393224 | tf_op jit(solution)/shard_map/ppermute | solution.py:38
  85.0 8.7 %collective-permute-start.25 = (bf16[128,512]{1,0:T(8,128)(2,1)S(1)}, bf16[128,512]{1,0:T(8,128)(2,1)S(1)}, u32[]{:S(2)}, u32[]{:S(2)}) collective-permute-start(bf16[128,512]{1,0:T(8,128)(2,1)S(1)} %fusion.10), channel_id=1, source_target_pairs={{0,24},{1,25},{2,26},{3,27},{4,28},{5,29},{6,30},{7,31},{8,16},{9,... | collective-permute-start | bytes 393224 | tf_op jit(solution)/shard_map/ppermute | solution.py:38
  88.5 7.3 %collective-permute-start.19 = (bf16[128,512]{1,0:T(8,128)(2,1)S(1)}, bf16[128,512]{1,0:T(8,128)(2,1)S(1)}, u32[]{:S(2)}, u32[]{:S(2)}) collective-permute-start(bf16[128,512]{1,0:T(8,128)(2,1)S(1)} %fusion.11), channel_id=1, source_target_pairs={{0,16},{1,17},{2,18},{3,19},{4,20},{5,21},{6,22},{7,23},{8,24},{9,... | collective-permute-start | bytes 393224 | tf_op jit(solution)/shard_map/ppermute | solution.py:38
  89.4 6.5 %collective-permute-start.13 = (bf16[128,512]{1,0:T(8,128)(2,1)}, bf16[128,512]{1,0:T(8,128)(2,1)S(1)}, u32[]{:S(2)}, u32[]{:S(2)}) collective-permute-start(bf16[128,512]{1,0:T(8,128)(2,1)} %fusion.12), channel_id=1, source_target_pairs={{0,8},{1,9},{2,10},{3,11},{4,12},{5,13},{6,14},{7,15},{8,0},{9,1},... | collective-permute-start | bytes 393224 | tf_op jit(solution)/shard_map/ppermute | solution.py:38
  (3 other events, 3.6 us)
